TPU v7x, 32 devices: a whole 2x2x4 slice. The times are simulated.
32 devices in a mesh: kv: 8 (over z, y), tp: 4 (over x, core).
Axes of the slice: x: 2, y: 2, z: 4, core: 2. Of those that a mesh axis runs over, the one named last changes fastest.
Arguments:
- tokens: bfloat16 [128, 4096], P('tp', 'kv')
- seq_pos: int32 [128], P('kv'), may hold values from 0 to 4095
- state: float32 [128, 16, 128, 256], P('kv', 'tp'), may hold values from -0.6 to 0.6
- norm_in_gain: float32 [4096], P('kv'), may hold values from 0.1 to 1.9
- query_weight: bfloat16 [4096, 2048], P('kv', 'tp'), may hold values from -0.09375 to 0.09375
- key_weight: bfloat16 [4096, 2048], P('kv', 'tp'), may hold values from -0.09375 to 0.09375
- value_weight: bfloat16 [4096, 4096], P('kv', 'tp'), may hold values from -0.09375 to 0.09375
- gate_weight: bfloat16 [4096, 4096], P('kv', 'tp'), may hold values from -0.09375 to 0.09375
- head_gain: float32 [4096], P('tp'), may hold values from 0.1 to 1.9
- out_weight: bfloat16 [4096, 4096], P('tp', 'kv'), may hold values from -0.09375 to 0.09375
- norm_mlp_gain: float32 [4096], P('kv'), may hold values from 0.1 to 1.9
- hidden_weight: bfloat16 [4096, 16384], P('kv', 'tp'), may hold values from -0.09375 to 0.09375
- down_weight: bfloat16 [16384, 4096], P('tp', 'kv'), may hold values from -0.046875 to 0.046875
Outputs:
- output: bfloat16 [128, 4096], P('tp', 'kv')
- new_state: float32 [128, 16, 128, 256], P('kv', 'tp')
All inputs are finite; a program needn't handle non-finite values.
Results may differ from a plain program's by a relative error of at most 0.03.
Values may be sent and summed in bfloat16 or wider, within the bound.
A program may use at most 64 MiB of HBM per device.

v0:
```python
import jax
import jax.numpy as jnp
from jax import lax
from jax.sharding import PartitionSpec as P

D = 4096
H = 16
DK = 128
DV = 256


EPS = 1e-06


def rotate(vectors, positions):
    half = vectors.shape[-1] // 2
    inverse = jnp.power(10000.0, -jnp.arange(half, dtype=jnp.float32) / half)
    angles = positions.astype(jnp.float32)[:, None] * inverse[None, :]
    cosine = jnp.cos(angles)[:, None, :]
    sine = jnp.sin(angles)[:, None, :]
    first, second = (vectors[..., :half], vectors[..., half:])
    return jnp.concatenate(
        [first * cosine - second * sine, first * sine + second * cosine], axis=-1
    )


def head_decay(head_ids):
    return 1.0 - jnp.exp2(-2.0 - 6.0 * head_ids / (H - 1))


def local(
    tokens,
    seq_pos,
    state,
    norm_in_gain,
    query_weight,
    key_weight,
    value_weight,
    gate_weight,
    head_gain,
    out_weight,
    norm_mlp_gain,
    hidden_weight,
    down_weight,
):
    rows_all = lax.all_gather(tokens, "tp", axis=0, tiled=True)
    rows_f = rows_all.astype(jnp.float32)
    squares_in = jnp.sum(rows_f * rows_f, axis=1)
    normed_in = (rows_f * norm_in_gain[None, :]).astype(jnp.bfloat16)
    term_query = jnp.dot(normed_in, query_weight, preferred_element_type=jnp.float32).astype(
        jnp.bfloat16
    )
    term_keys = jnp.dot(normed_in, key_weight, preferred_element_type=jnp.float32).astype(
        jnp.bfloat16
    )
    term_values = jnp.dot(normed_in, value_weight, preferred_element_type=jnp.float32).astype(
        jnp.bfloat16
    )
    term_gates = jnp.dot(normed_in, gate_weight, preferred_element_type=jnp.float32).astype(
        jnp.bfloat16
    )
    total_all = lax.psum(squares_in, "kv")
    query, keys, values, gates = (
        lax.psum_scatter(term_query, "kv", scatter_dimension=0, tiled=True).astype(jnp.float32),
        lax.psum_scatter(term_keys, "kv", scatter_dimension=0, tiled=True).astype(jnp.float32),
        lax.psum_scatter(term_values, "kv", scatter_dimension=0, tiled=True).astype(jnp.float32),
        lax.psum_scatter(term_gates, "kv", scatter_dimension=0, tiled=True).astype(jnp.float32),
    )
    own_rows = query.shape[0]
    total_in = lax.dynamic_slice_in_dim(total_all, lax.axis_index("kv") * own_rows, own_rows, 0)
    factor = lax.rsqrt(total_in / D + EPS)[:, None]
    query, keys, values, gates = (query * factor, keys * factor, values * factor, gates * factor)
    local_rows = query.shape[0]
    heads_dev = H // lax.axis_size("tp")
    turned_query = rotate(query.reshape(local_rows, heads_dev, DK), seq_pos)
    turned_keys = rotate(keys.reshape(local_rows, heads_dev, DK), seq_pos) * DK ** (-0.5)
    head_ids = (lax.axis_index("tp") * heads_dev + jnp.arange(heads_dev, dtype=jnp.int32)).astype(
        jnp.float32
    )
    decay = head_decay(head_ids)
    new_state = decay[None, :, None, None] * state + jnp.einsum(
        "bhk,bhv->bhkv",
        turned_keys,
        values.reshape(local_rows, heads_dev, DV),
        precision=lax.Precision.HIGHEST,
    )
    read = jnp.einsum("bhk,bhkv->bhv", turned_query, new_state, precision=lax.Precision.HIGHEST)
    read = read * lax.rsqrt(jnp.mean(read * read, axis=-1, keepdims=True) + EPS)
    mixed = (
        read.reshape(local_rows, heads_dev * DV) * head_gain[None, :] * jax.nn.silu(gates)
    ).astype(jnp.bfloat16)
    attn_terms = jnp.dot(
        lax.all_gather(mixed, "kv", axis=0, tiled=True),
        out_weight,
        preferred_element_type=jnp.float32,
    )
    attn = lax.psum_scatter(
        attn_terms.astype(jnp.bfloat16), "tp", scatter_dimension=0, tiled=True
    ).astype(jnp.float32)
    resid = (tokens.astype(jnp.float32) + attn).astype(jnp.bfloat16)
    resid_all = lax.all_gather(resid, "tp", axis=0, tiled=True)
    resid_f = resid_all.astype(jnp.float32)
    squares_mid = jnp.sum(resid_f * resid_f, axis=1)
    normed_mid = (resid_f * norm_mlp_gain[None, :]).astype(jnp.bfloat16)
    term_hidden = jnp.dot(normed_mid, hidden_weight, preferred_element_type=jnp.float32).astype(
        jnp.bfloat16
    )
    total_mid = lax.psum(squares_mid, "kv")
    scale_mid = lax.rsqrt(total_mid / D + EPS)[:, None]
    hidden = lax.psum(term_hidden, "kv").astype(jnp.float32)
    active = jnp.square(jax.nn.relu(hidden * scale_mid)).astype(jnp.bfloat16)
    down_terms = jnp.dot(active, down_weight, preferred_element_type=jnp.float32)
    down = lax.psum_scatter(
        down_terms.astype(jnp.bfloat16), "tp", scatter_dimension=0, tiled=True
    ).astype(jnp.float32)
    output = (resid.astype(jnp.float32) + down).astype(jnp.bfloat16)
    return (output, new_state)


def solution(mesh):
    placed = (
        P("tp", "kv"),
        P("kv"),
        P("kv", "tp", None, None),
        P("kv"),
        P("kv", "tp"),
        P("kv", "tp"),
        P("kv", "tp"),
        P("kv", "tp"),
        P("tp"),
        P("tp", "kv"),
        P("kv"),
        P("kv", "tp"),
        P("tp", "kv"),
    )
    return jax.shard_map(
        local,
        mesh=mesh,
        in_specs=placed,
        out_specs=(P("tp", "kv"), P("kv", "tp", None, None)),
        check_vma=False,
    )
```

profile of v0, /device:TPU:0, one launch (start us, length us, event | category | flops | bytes accessed | tf_op | source)
XLA Modules:
  0.0 445.5 jit_solution(3664040884219889815)
XLA Ops:
  7.2 6.9 %all_gather.9 = bf16[128,512]{1,0:T(8,128)(2,1)S(1)} all-gather(bf16[32,512]{1,0:T(8,128)(2,1)} %param.13), channel_id=1, replica_groups=mesh['kv'=8,'tp'=4] {'tp'}, dimensions={0}, use_global_device_ids=true | all-gather | bytes 163840 | tf_op jit(solution)/shard_map/all_gather | solution.py:46
  14.1 2.0 convolution_convert_fusion.4
  16.1 1.9 convolution_convert_fusion.5
  18.1 1.7 convolution_convert_fusion.2
  19.9 2.2 convolution_convert_fusion.1
  22.3 0.1 fusion.3
  22.4 22.1 %psum.21 = f32[128]{0:T(128)S(1)} all-reduce(f32[128]{0:T(128)S(1)} %fusion.3), channel_id=1, replica_groups=mesh['kv'=8,'tp'=4] {'kv'}, use_global_device_ids=true, to_apply=%region_2.0 | all-reduce | flops 128 | bytes 1024 | tf_op jit(solution)/shard_map/psum | solution.py:62
  44.5 0.1 multiply_cosine_fusion
  44.7 35.0 %reduce-scatter.9.cloned.1.call-done = bf16[16,512]{1,0:T(8,128)(2,1)} async-done(((bf16[128,512]{1,0:T(8,128)(2,1)}), bf16[16,512]{1,0:T(8,128)(2,1)}) %reduce-scatter.9.cloned.1.call-update) | async-done | bytes 16400 | tf_op jit(solution)/shard_map/reduce_scatter | solution.py:65
  79.7 64.2 %reduce-scatter.7.cloned.1.call-done = bf16[16,512]{1,0:T(8,128)(2,1)} async-done(((bf16[128,512]{1,0:T(8,128)(2,1)}), bf16[16,512]{1,0:T(8,128)(2,1)}) %reduce-scatter.7.cloned.1.call-update) | async-done | bytes 16400 | tf_op jit(solution)/shard_map/reduce_scatter | solution.py:64
  143.9 0.8 convert_multiply_fusion.5
  144.7 0.1 multiply_subtract_fusion
  144.8 0.1 pad_maximum_fusion
  144.9 64.0 %reduce-scatter.11.cloned.1.call-done = bf16[16,1024]{1,0:T(8,128)(2,1)} async-done(((bf16[128,1024]{1,0:T(8,128)(2,1)}), bf16[16,1024]{1,0:T(8,128)(2,1)}) %reduce-scatter.11.cloned.1.call-update) | async-done | bytes 32784 | tf_op jit(solution)/shard_map/reduce_scatter | solution.py:66
  208.9 0.8 convert_multiply_fusion.4
  209.7 4.1 multiply_add_fusion
  213.9 4.1 fusion.14
  218.0 0.1 fusion.12
  218.3 55.3 %reduce-scatter.13.cloned.1.call-done = bf16[16,1024]{1,0:T(8,128)(2,1)} async-done(((bf16[128,1024]{1,0:T(8,128)(2,1)}), bf16[16,1024]{1,0:T(8,128)(2,1)}) %reduce-scatter.13.cloned.1.call-update) | async-done | bytes 32784 | tf_op jit(solution)/shard_map/reduce_scatter | solution.py:67
  273.6 0.9 multiply_convert_fusion.2
  274.4 30.9 %all_gather.10 = bf16[128,1024]{1,0:T(8,128)(2,1)S(1)} all-gather(bf16[16,1024]{1,0:T(8,128)(2,1)S(1)} %multiply_convert_fusion.2), channel_id=1, replica_groups=mesh['kv'=8,'tp'=4] {'kv'}, dimensions={0}, use_global_device_ids=true | all-gather | bytes 294912 | tf_op jit(solution)/shard_map/all_gather | solution.py:93
  305.3 1.0 convolution_convert_fusion.6
  306.4 18.8 %reduce-scatter.15.cloned.1.call-done = bf16[32,512]{1,0:T(8,128)(2,1)} async-done(((bf16[128,512]{1,0:T(8,128)(2,1)}), bf16[32,512]{1,0:T(8,128)(2,1)}) %reduce-scatter.15.cloned.1.call-update) | async-done | bytes 32784 | tf_op jit(solution)/shard_map/reduce_scatter | solution.py:97
  325.2 0.8 add_convert_fusion.1
  325.9 5.4 %all_gather.11 = bf16[128,512]{1,0:T(8,128)(2,1)S(1)} all-gather(bf16[32,512]{1,0:T(8,128)(2,1)S(1)} %add_convert_fusion.1), channel_id=1, replica_groups=mesh['kv'=8,'tp'=4] {'tp'}, dimensions={0}, use_global_device_ids=true | all-gather | bytes 163840 | tf_op jit(solution)/shard_map/all_gather | solution.py:101
  331.3 3.9 convolution_convert_fusion
  335.4 0.1 fusion.5
  335.5 21.6 %psum.23 = f32[128]{0:T(128)S(1)} all-reduce(f32[128]{0:T(128)S(1)} %fusion.5), channel_id=1, replica_groups=mesh['kv'=8,'tp'=4] {'kv'}, use_global_device_ids=true, to_apply=%region_10.11 | all-reduce | flops 128 | bytes 1024 | tf_op jit(solution)/shard_map/psum | solution.py:108
  357.1 56.9 %all-reduce.2.cloned.1.call-done = bf16[128,4096]{1,0:T(8,128)(2,1)} async-done(((bf16[128,4096]{1,0:T(8,128)(2,1)}), bf16[128,4096]{1,0:T(8,128)(2,1)}) %all-reduce.2.cloned.1.call-update) | async-done | bytes 1048592 | tf_op jit(solution)/shard_map/psum | solution.py:110
  414.0 3.9 convolution_convert_fusion.3
  417.9 19.4 %reduce-scatter.17.cloned.1.call-done = bf16[32,512]{1,0:T(8,128)(2,1)} async-done(((bf16[128,512]{1,0:T(8,128)(2,1)}), bf16[32,512]{1,0:T(8,128)(2,1)}) %reduce-scatter.17.cloned.1.call-update) | async-done | bytes 32784 | tf_op jit(solution)/shard_map/reduce_scatter | solution.py:113
  437.3 1.4 add_convert_fusion
  (39 shorter events, 0.7 us)
Async XLA Ops:
  7.2 11.0 %copy-start = (bf16[512,1024]{1,0:T(8,128)(2,1)S(1)}, bf16[512,1024]{1,0:T(8,128)(2,1)}, u32[]{:S(2)}) copy-start(bf16[512,1024]{1,0:T(8,128)(2,1)} %param.19) | copy-start | bytes 3145732
  7.2 15.2 %copy-start.6 = (s32[16]{0:T(128)S(1)}, s32[16]{0:T(128)}, u32[]{:S(2)}) copy-start(s32[16]{0:T(128)} %param.14) | copy-start | bytes 196
  7.2 72.5 %reduce-scatter.9.cloned.1.call-start = ((), (), s32[]{:S(2)}) async-start(), calls=%async_computation.7 | async-start | bytes 147456 | tf_op jit(solution)/shard_map/reduce_scatter | solution.py:65
  16.1 127.8 %reduce-scatter.7.cloned.1.call-start = ((), (), s32[]{:S(2)}) async-start(), calls=%async_computation.6 | async-start | bytes 147456 | tf_op jit(solution)/shard_map/reduce_scatter | solution.py:64
  18.1 190.8 %reduce-scatter.11.cloned.1.call-start = ((), (), s32[]{:S(2)}) async-start(), calls=%async_computation.8 | async-start | bytes 294912 | tf_op jit(solution)/shard_map/reduce_scatter | solution.py:66
  19.9 253.7 %reduce-scatter.13.cloned.1.call-start = ((), (), s32[]{:S(2)}) async-start(), calls=%async_computation.9 | async-start | bytes 294912 | tf_op jit(solution)/shard_map/reduce_scatter | solution.py:67
  22.2 303.0 %reduce-scatter.15.cloned.1.call-start = ((), (), s32[]{:S(2)}) async-start(), calls=%async_computation.10 | async-start | bytes 163840 | tf_op jit(solution)/shard_map/reduce_scatter | solution.py:97
  213.9 4.1 copy-start.1
  213.9 59.7 %copy-start.4 = (f32[1024]{0:T(1024)S(1)}, f32[1024]{0:T(1024)}, u32[]{:S(2)}) copy-start(f32[1024]{0:T(1024)} %param.21) | copy-start | bytes 12292
  213.9 91.4 %copy-start.2 = (bf16[1024,512]{1,0:T(8,128)(2,1)S(1)}, bf16[1024,512]{1,0:T(8,128)(2,1)}, u32[]{:S(2)}) copy-start(bf16[1024,512]{1,0:T(8,128)(2,1)} %param.22) | copy-start | bytes 3145732
  213.9 111.2 %copy-start.3 = (bf16[32,512]{1,0:T(8,128)(2,1)S(1)}, bf16[32,512]{1,0:T(8,128)(2,1)}, u32[]{:S(2)}) copy-start(bf16[32,512]{1,0:T(8,128)(2,1)} %param.13) | copy-start | bytes 98308
  213.9 117.4 %copy-start.5 = (f32[512]{0:T(512)S(1)}, f32[512]{0:T(512)}, u32[]{:S(2)}) copy-start(f32[512]{0:T(512)} %param.23) | copy-start | bytes 6148
  306.3 107.6 %all-reduce.2.cloned.1.call-start = ((), (), s32[]{:S(2)}) async-start(), calls=%async_computation.11 | async-start | bytes 2097152 | tf_op jit(solution)/shard_map/psum | solution.py:110
  335.3 102.0 %reduce-scatter.17.cloned.1.call-start = ((), (), s32[]{:S(2)}) async-start(), calls=%async_computation.12 | async-start | bytes 163840 | tf_op jit(solution)/shard_map/reduce_scatter | solution.py:113
Sparse Core Ops, SparseCore 0:
  16.2 63.4 reduce-scatter.8
  83.0 60.8 reduce-scatter.6
  147.8 61.0 reduce-scatter.10
  212.1 61.4 reduce-scatter.12
  306.5 18.6 reduce-scatter.14
  335.4 78.4 all-reduce.1
  418.0 19.2 reduce-scatter.16
where the time goes:
time: 446 us
  waiting for transfers between devices  314 us (70%)
  blocking collectives  86.9 us (19%)
  matrix products  20.8 us (5%)
  between operations  14.3 us (3%)
  other arithmetic  9.62 us (2%)
    reduce_scatter x1, waiting for transfers between devices, local(): lax.psum_scatter(term_query, 'kv', scatter_dimension=0, tiled=True)  64.2 us
    reduce_scatter x1, waiting for transfers between devices, local(): lax.psum_scatter(term_values, 'kv', scatter_dimension=0, tiled=True)  64 us
    psum x1, waiting for transfers between devices, local(): hidden = lax.psum(term_hidden, 'kv').astype(jnp.float32)  56.9 us
    reduce_scatter x1, waiting for transfers between devices, local(): lax.psum_scatter(term_gates, 'kv', scatter_dimension=0, tiled=True)  55.3 us
    reduce_scatter x1, waiting for transfers between devices, local(): lax.psum_scatter(term_keys, 'kv', scatter_dimension=0, tiled=True)  35 us
    all_gather x1, blocking collectives, local(): lax.all_gather(mixed, 'kv', axis=0, tiled=True)  30.9 us
    psum x1, blocking collectives, local(): total_all = lax.psum(squares_in, 'kv')  22.1 us
    psum x1, blocking collectives, local(): total_mid = lax.psum(squares_mid, 'kv')  21.6 us
  transfers between devices with their start and end apart: 7, of which 7 were waited for; matrix products, arithmetic and copies ran while one was open for 4% of the time, Pallas kernels for 0%

commit v1 on v0

v1 whole, which is shorter than its diff:
```python
import functools

import jax
import jax.numpy as jnp
from jax import lax
from jax.experimental import pallas as pl
from jax.experimental.pallas import tpu as pltpu
from jax.sharding import PartitionSpec as P

H = 16
DK = 128
DV = 256
EPS = 1e-06
MESH = pl.DeviceIdType.MESH
VMEM = pltpu.VMEM
DMA = pltpu.SemaphoreType.DMA


def remote(src, dst, send, recv, where):
    return pltpu.make_async_remote_copy(
        src_ref=src, dst_ref=dst, send_sem=send, recv_sem=recv, device_id=where, device_id_type=MESH
    )


def entry_barrier(n_kv, n_tp):
    barrier = pltpu.get_barrier_semaphore()
    for axis, n in (("kv", n_kv), ("tp", n_tp)):
        me = lax.axis_index(axis)
        for k in range(1, n):
            pl.semaphore_signal(
                barrier, inc=1, device_id={axis: lax.rem(me + k, n)}, device_id_type=MESH
            )
    pl.semaphore_wait(barrier, n_kv + n_tp - 2)


def gather_tp(own, rows, send, recv, n):
    me = lax.axis_index("tp")
    copies = [
        remote(own, rows.at[me], send.at[k], recv.at[k], {"tp": lax.rem(me + k, n)})
        for k in range(1, n)
    ]
    for copy in copies:
        copy.start()
    rows[me] = own[...]
    for copy in copies:
        copy.wait_recv()
    return copies


def reduce_tp(terms, landed, send, recv, n):
    me = lax.axis_index("tp")
    copies = []
    for k in range(1, n):
        to = lax.rem(me + k, n)
        copies.append(remote(terms.at[to], landed.at[k], send.at[k], recv.at[k], {"tp": to}))
    for copy in copies:
        copy.start()
    total = terms[me].astype(jnp.float32)
    for k, copy in enumerate(copies, 1):
        copy.wait_recv()
        total += landed[k].astype(jnp.float32)
    return total, copies


def squares_start(squares, landed, send, recv, n):
    me = lax.axis_index("kv")
    copies = []
    for k in range(1, n):
        to = lax.rem(me + k, n)
        copies.append(remote(squares.at[to], landed.at[k], send.at[k], recv.at[k], {"kv": to}))
    for copy in copies:
        copy.start()
    return copies


def squares_total(copies, squares, landed):
    total = squares[lax.axis_index("kv")]
    for k, copy in enumerate(copies, 1):
        copy.wait_recv()
        total += landed[k]
    return total[:, :1]


class Scatter:
    def __init__(self, terms, land_in, partial, land_out, sems, outer, inner):
        self.terms, self.land_in, self.partial, self.land_out = terms, land_in, partial, land_out
        me = lax.axis_index("kv")
        self.o, self.i = me // inner, lax.rem(me, inner)
        self.outer, self.inner = outer, inner
        send_in, recv_in, send_out, recv_out = sems
        self.first, self.second = {}, {}
        for s in self.order():
            to_o = lax.rem(self.o + s, outer)
            for k in range(1, inner):
                to_i = lax.rem(self.i + k, inner)
                self.first[s, k] = remote(
                    terms.at[to_o, to_i],
                    land_in.at[k, s],
                    send_in.at[k, s],
                    recv_in.at[k, s],
                    {"kv": self.o * inner + to_i},
                )
            if s:
                source = partial.at[s] if inner > 1 else terms.at[to_o, self.i]
                self.second[s] = remote(
                    source,
                    land_out.at[s],
                    send_out.at[s],
                    recv_out.at[s],
                    {"kv": to_o * inner + self.i},
                )

    def order(self):
        return list(range(1, self.outer)) + [0]

    def start(self):
        for copy in self.first.values():
            copy.start()

    def middle(self):
        for s in self.order():
            to_o = lax.rem(self.o + s, self.outer)
            if self.inner > 1:
                total = self.terms[to_o, self.i].astype(jnp.float32)
                for k in range(1, self.inner):
                    self.first[s, k].wait_recv()
                    total += self.land_in[k, s].astype(jnp.float32)
                self.partial[s] = total.astype(jnp.bfloat16)
            if s:
                self.second[s].start()

    def arrived(self):
        for copy in self.second.values():
            copy.wait_recv()

    def total(self, columns):
        if self.inner > 1:
            total = self.partial[0, :, columns].astype(jnp.float32)
        else:
            total = self.terms[self.o, self.i, :, columns].astype(jnp.float32)
        for s in range(1, self.outer):
            total += self.land_out[s, :, columns].astype(jnp.float32)
        return total

    def copies(self):
        return list(self.first.values()) + list(self.second.values())


class Gather:
    def __init__(self, held, sems, outer, inner):
        me = lax.axis_index("kv")
        o, i = me // inner, lax.rem(me, inner)
        send_out, recv_out, send_in, recv_in = sems
        self.outer, self.inner = outer, inner
        self.first, self.second = {}, {}
        for s in range(outer):
            if s:
                self.first[s] = remote(
                    held.at[o, i],
                    held.at[o, i],
                    send_out.at[s],
                    recv_out.at[s],
                    {"kv": lax.rem(o + s, outer) * inner + i},
                )
            origin = lax.rem(o + outer - s, outer)
            for k in range(1, inner):
                self.second[s, k] = remote(
                    held.at[origin, i],
                    held.at[origin, i],
                    send_in.at[k, s],
                    recv_in.at[k, s],
                    {"kv": o * inner + lax.rem(i + k, inner)},
                )

    def run(self):
        for copy in self.first.values():
            copy.start()
        for s in range(self.outer):
            if s:
                self.first[s].wait_recv()
            for k in range(1, self.inner):
                self.second[s, k].start()
        for copy in self.second.values():
            copy.wait_recv()

    def copies(self):
        return list(self.first.values()) + list(self.second.values())


def project_kernel(
    n_kv, n_tp, inner, features,
    tokens, gain, cosine, sine, wq, wk, wv, wg,
    qk_out, v_out, g_out,
    rows, weights, terms, land_in, partial, land_out, squares, squares_in,
    w_sem, tp_send, tp_recv, sq_send, sq_recv, s1, r1, s2, r2,
):
    outer = n_kv // inner
    own = cosine.shape[0]
    loads, offset = [], 0
    for index, ref in enumerate((wq, wk, wv, wg)):
        width = ref.shape[1]
        part = pl.ds(offset, width)
        loads.append((pltpu.make_async_copy(ref, weights.at[:, part], w_sem.at[index]), offset, width))
        offset += width
    for load, _, _ in loads:
        load.start()
    entry_barrier(n_kv, n_tp)
    pending = gather_tp(tokens, rows, tp_send, tp_recv, n_tp)
    batch = rows.shape[0] * rows.shape[1]
    x = rows[...].reshape(batch, rows.shape[2]).astype(jnp.float32)
    total = jnp.sum(x * x, axis=1, keepdims=True)
    squares[...] = jnp.broadcast_to(total, (batch, 128)).reshape(n_kv, own, 128)
    sq_copies = squares_start(squares, squares_in, sq_send, sq_recv, n_kv)
    normed = (x * gain[...]).astype(jnp.bfloat16)
    for load, offset, width in loads:
        load.wait()
        term = jnp.dot(
            normed, weights[:, offset : offset + width], preferred_element_type=jnp.float32
        ).astype(jnp.bfloat16)
        terms[:, :, :, offset : offset + width] = term.reshape(outer, inner, own, width)
    scatter = Scatter(terms, land_in, partial, land_out, (s1, r1, s2, r2), outer, inner)
    scatter.start()
    scatter.middle()
    scale = lax.rsqrt(squares_total(sq_copies, squares, squares_in) / features + EPS)
    scatter.arrived()
    c, s = cosine[...], sine[...]
    heads = wq.shape[1] // DK
    for h in range(2 * heads):
        vec = scatter.total(pl.ds(h * DK, DK)) * scale
        turned = vec * c + pltpu.roll(vec, DK // 2, 1) * s
        if h >= heads:
            turned = turned * DK ** (-0.5)
        qk_out[:, h, :] = turned
    for h in range(heads):
        v_out[:, h, :] = scatter.total(pl.ds(2 * heads * DK + h * DV, DV)) * scale
        g_out[:, h, :] = scatter.total(pl.ds(heads * (2 * DK + DV) + h * DV, DV)) * scale
    for copy in pending + sq_copies + scatter.copies():
        copy.wait_send()


def state_kernel(qk, v, g, gain, state, new_state, mixed, acc):
    heads = state.shape[1]
    b = pl.program_id(0)
    columns = qk[0].T
    first = lax.axis_index("tp") * heads
    for h in range(heads):
        ids = jnp.full((1, DV), first + h, jnp.int32).astype(jnp.float32)
        decay = 1.0 - jnp.exp2(-2.0 - 6.0 * ids / (H - 1))
        query = columns[:, h : h + 1]
        key = columns[:, heads + h : heads + h + 1]
        new = decay * state[0, h] + key * v[0, h : h + 1, :]
        new_state[0, h] = new
        read = jnp.sum(query * new, axis=0, keepdims=True)
        read = read * lax.rsqrt(jnp.mean(read * read, axis=-1, keepdims=True) + EPS)
        gate = g[0, h : h + 1, :]
        part = slice(h * DV, (h + 1) * DV)
        acc[pl.ds(b, 1), part] = read * gain[:, part] * (gate / (1.0 + jnp.exp(-gate)))

    @pl.when(b == pl.num_programs(0) - 1)
    def _():
        mixed[...] = acc[...].astype(jnp.bfloat16)


def mixer_kernel(
    n_kv, n_tp, inner, features, wide,
    mixed, tokens, gain, w_out, w_hidden, w_down,
    output,
    held, wo, wh, wd, out_terms, out_land, resid, rows, squares, squares_in,
    terms, land_in, partial, land_out, active, acc, down_terms, down_land,
    w_sem, gs1, gr1, gs2, gr2, os, orr, ts, tr, qs, qr, s1, r1, s2, r2, hs1, hr1, hs2, hr2, ds, dr,
):
    outer = n_kv // inner
    own, width = mixed.shape
    me = lax.axis_index("kv")
    loads = [
        pltpu.make_async_copy(w_out, wo, w_sem.at[0]),
        pltpu.make_async_copy(w_hidden, wh, w_sem.at[1]),
        pltpu.make_async_copy(w_down, wd, w_sem.at[2]),
    ]
    for load in loads:
        load.start()
    o, i = me // inner, lax.rem(me, inner)
    held[o, i] = mixed[...]
    entry_barrier(n_kv, n_tp)
    gather = Gather(held, (gs1, gr1, gs2, gr2), outer, inner)
    gather.run()
    pending = gather.copies()
    loads[0].wait()
    batch = n_kv * own
    piece = batch // n_tp
    cols = wo.shape[1]
    out_terms[...] = (
        jnp.dot(held[...].reshape(batch, width), wo[...], preferred_element_type=jnp.float32)
        .astype(jnp.bfloat16)
        .reshape(n_tp, piece, cols)
    )
    attn, copies = reduce_tp(out_terms, out_land, os, orr, n_tp)
    pending += copies
    resid[...] = (tokens[...].astype(jnp.float32) + attn).astype(jnp.bfloat16)
    pending += gather_tp(resid, rows, ts, tr, n_tp)
    x = rows[...].reshape(batch, cols).astype(jnp.float32)
    total = jnp.sum(x * x, axis=1, keepdims=True)
    squares[...] = jnp.broadcast_to(total, (batch, 128)).reshape(n_kv, own, 128)
    sq_copies = squares_start(squares, squares_in, qs, qr, n_kv)
    pending += sq_copies
    normed = (x * gain[...]).astype(jnp.bfloat16)
    loads[1].wait()
    hidden = wh.shape[1]

    @pl.loop(0, hidden // wide)
    def _(c):
        part = pl.ds(pl.multiple_of(c * wide, wide), wide)
        term = jnp.dot(normed, wh[:, part], preferred_element_type=jnp.float32)
        terms[:, :, :, part] = term.astype(jnp.bfloat16).reshape(outer, inner, own, wide)

    scatter = Scatter(terms, land_in, partial, land_out, (s1, r1, s2, r2), outer, inner)
    scatter.start()
    scatter.middle()
    scale = lax.rsqrt(squares_total(sq_copies, squares, squares_in) / features + EPS)
    scatter.arrived()
    pending += scatter.copies()
    for c in range(hidden // wide):
        part = pl.ds(c * wide, wide)
        value = jnp.maximum(scatter.total(part) * scale, 0.0)
        active[o, i, :, part] = (value * value).astype(jnp.bfloat16)
    gather = Gather(active, (hs1, hr1, hs2, hr2), outer, inner)
    gather.run()
    pending += gather.copies()
    loads[2].wait()
    acc[...] = jnp.zeros_like(acc)

    @pl.loop(0, hidden // wide)
    def _(c):
        part = pl.ds(pl.multiple_of(c * wide, wide), wide)
        left = active[:, :, :, part].reshape(batch, wide)
        acc[...] += jnp.dot(left, wd[part, :], preferred_element_type=jnp.float32)

    down_terms[...] = acc[...].astype(jnp.bfloat16).reshape(n_tp, piece, cols)
    down, copies = reduce_tp(down_terms, down_land, ds, dr, n_tp)
    pending += copies
    output[...] = (resid[...].astype(jnp.float32) + down).astype(jnp.bfloat16)
    for copy in pending:
        copy.wait_send()


def local(
    n_kv, n_tp, inner, features,
    tokens, seq_pos, state, norm_in_gain, query_weight, key_weight, value_weight, gate_weight,
    head_gain, out_weight, norm_mlp_gain, hidden_weight, down_weight,
):
    outer = n_kv // inner
    f32, bf16 = jnp.float32, jnp.bfloat16
    half = DK // 2
    inverse = jnp.power(10000.0, -jnp.arange(half, dtype=f32) / half)
    angles = seq_pos.astype(f32)[:, None] * inverse[None, :]
    cos, sin = jnp.cos(angles), jnp.sin(angles)
    cosine = jnp.concatenate([cos, cos], axis=1)
    sine = jnp.concatenate([-sin, sin], axis=1)

    own = seq_pos.shape[0]
    piece, cols = tokens.shape
    heads = state.shape[1]
    whole = heads * 2 * (DK + DV)
    vmem, hbm = pl.BlockSpec(memory_space=VMEM), pl.BlockSpec(memory_space=pl.ANY)

    def scatter_buffers(width):
        return [
            VMEM((outer, inner, own, width), bf16),
            VMEM((inner, outer, own, width), bf16),
            VMEM((outer, own, width), bf16),
            VMEM((outer, own, width), bf16),
        ]

    two_in = [DMA((inner, outer)), DMA((inner, outer))]
    two_out = [DMA((outer,)), DMA((outer,))]
    over_tp = [DMA((n_tp,)), DMA((n_tp,))]
    over_kv = [DMA((n_kv,)), DMA((n_kv,))]
    qk, v, g = pl.pallas_call(
        functools.partial(project_kernel, n_kv, n_tp, inner, features),
        out_shape=[
            jax.ShapeDtypeStruct((own, 2 * heads, DK), f32),
            jax.ShapeDtypeStruct((own, heads, DV), f32),
            jax.ShapeDtypeStruct((own, heads, DV), f32),
        ],
        in_specs=[vmem] * 4 + [hbm] * 4,
        out_specs=[vmem] * 3,
        scratch_shapes=[VMEM((n_tp, piece, cols), bf16), VMEM((cols, whole), bf16)]
        + scatter_buffers(whole)
        + [VMEM((n_kv, own, 128), f32), VMEM((n_kv, own, 128), f32), DMA((4,))]
        + over_tp + over_kv + two_in + two_out,
        compiler_params=pltpu.CompilerParams(
            collective_id=0, has_side_effects=True, vmem_limit_bytes=48 * 2**20
        ),
    )(
        tokens, norm_in_gain[None, :], cosine, sine,
        query_weight, key_weight, value_weight, gate_weight,
    )

    def per_row(*shape):
        return pl.BlockSpec((1,) + shape, lambda b: (b,) + (0,) * len(shape))

    new_state, mixed = pl.pallas_call(
        state_kernel,
        grid=(own,),
        out_shape=[
            jax.ShapeDtypeStruct(state.shape, f32),
            jax.ShapeDtypeStruct((own, heads * DV), bf16),
        ],
        in_specs=[
            per_row(2 * heads, DK),
            per_row(heads, DV),
            per_row(heads, DV),
            pl.BlockSpec((1, heads * DV), lambda b: (0, 0)),
            per_row(heads, DK, DV),
        ],
        out_specs=[per_row(heads, DK, DV), pl.BlockSpec((own, heads * DV), lambda b: (0, 0))],
        scratch_shapes=[VMEM((own, heads * DV), f32)],
    )(qk, v, g, head_gain[None, :], state)

    hidden = hidden_weight.shape[1]
    wide = min(512, hidden)
    output = pl.pallas_call(
        functools.partial(mixer_kernel, n_kv, n_tp, inner, features, wide),
        out_shape=jax.ShapeDtypeStruct(tokens.shape, bf16),
        in_specs=[vmem] * 3 + [hbm] * 3,
        out_specs=vmem,
        scratch_shapes=[
            VMEM((outer, inner, own, heads * DV), bf16),
            VMEM(out_weight.shape, bf16),
            VMEM(hidden_weight.shape, bf16),
            VMEM(down_weight.shape, bf16),
            VMEM((n_tp, piece, cols), bf16),
            VMEM((n_tp, piece, cols), bf16),
            VMEM((piece, cols), bf16),
            VMEM((n_tp, piece, cols), bf16),
            VMEM((n_kv, own, 128), f32),
            VMEM((n_kv, own, 128), f32),
        ]
        + scatter_buffers(hidden)
        + [
            VMEM((outer, inner, own, hidden), bf16),
            VMEM((n_tp * piece, cols), f32),
            VMEM((n_tp, piece, cols), bf16),
            VMEM((n_tp, piece, cols), bf16),
            DMA((3,)),
        ]
        + two_out + two_in
        + over_tp + over_tp + over_kv
        + two_in + two_out
        + two_out + two_in
        + over_tp,
        compiler_params=pltpu.CompilerParams(
            collective_id=1, has_side_effects=True, vmem_limit_bytes=48 * 2**20
        ),
    )(mixed, tokens, norm_mlp_gain[None, :], out_weight, hidden_weight, down_weight)
    return output, new_state


def inner_size(mesh):
    column = mesh.devices[:, 0] if mesh.axis_names[0] == "kv" else mesh.devices[0, :]
    heights = [getattr(device, "coords", (0, 0, at))[2] for at, device in enumerate(column)]
    count = 1
    while count < len(heights) and heights[count] == heights[0]:
        count += 1
    return count if len(heights) % count == 0 else 1


def solution(mesh):
    n_kv, n_tp = mesh.shape["kv"], mesh.shape["tp"]
    inner = inner_size(mesh)
    placed = (
        P("tp", "kv"), P("kv"), P("kv", "tp", None, None), P("kv"),
        P("kv", "tp"), P("kv", "tp"), P("kv", "tp"), P("kv", "tp"),
        P("tp"), P("tp", "kv"), P("kv"), P("kv", "tp"), P("tp", "kv"),
    )

    def step(*args):
        return local(n_kv, n_tp, inner, args[0].shape[1] * n_kv, *args)

    return jax.shard_map(
        step, mesh=mesh, in_specs=placed,
        out_specs=(P("tp", "kv"), P("kv", "tp", None, None)), check_vma=False,
    )
```

time: 446 us -> 115 us (0.26)
  waiting for transfers between devices: 314 us -> 0 us
  Pallas kernels: 0 us -> 99.9 us
  blocking collectives: 86.9 us -> 0 us
  matrix products: 20.8 us -> 0 us
  between operations: 14.3 us -> 0.71 us
  local copies, waits for them, and re-layouts: 0.12 us -> 11.4 us
  other arithmetic: 9.62 us -> 0.88 us
    reduce_scatter x6 -> x0, waiting for transfers between devices: 257 us -> none  [the longest x1 64.2 us: local(): lax.psum_scatter(term_query, 'kv', scatter_dimension=0, tiled=True)]
    pallas_call x0 -> x3, Pallas kernels: none -> 99.9 us  [the longest x1 59.5 us: local(): pl.pallas_call(functools.partial(mixer_kernel, n_kv, n_tp, inner, feature...]
    psum x1 -> x0, waiting for transfers between devices: 56.9 us -> none  [local(): hidden = lax.psum(term_hidden, 'kv').astype(jnp.float32)]
    psum x2 -> x0, blocking collectives: 43.7 us -> none  [the longest x1 22.1 us: local(): total_all = lax.psum(squares_in, 'kv')]
    all_gather x3 -> x0, blocking collectives: 43.2 us -> none  [the longest x1 30.9 us: local(): lax.all_gather(mixed, 'kv', axis=0, tiled=True)]
    dot_general x8 -> x0, matrix products: 20.8 us -> none  [the longest x1 4.09 us: local(): jnp.einsum('bhk,bhkv->bhv', turned_query, new_state, precision=lax.Precis...]
    unnamed x15 -> x29, local copies, waits for them, and re-layouts: 0.06 us -> 11.4 us
  transfers between devices with their start and end apart: 7 -> 0, of which waited for: 7 -> 0; matrix products, arithmetic and copies ran while one was open for 4% -> 0% of each run, Pallas kernels for 0% -> 0%
where the time goes in v1:
time: 115 us; the launch traced here: 113 us
  Pallas kernels  99.9 us (87%)
  local copies, waits for them, and re-layouts  11.4 us (10%)
    pallas_call x1, Pallas kernels, local(): pl.pallas_call(functools.partial(mixer_kernel, n_kv, n_tp, inner, feature...  59.5 us
    pallas_call x1, Pallas kernels, local(): pl.pallas_call(functools.partial(project_kernel, n_kv, n_tp, inner, featu...  25.2 us
    pallas_call x1, Pallas kernels, local(): pl.pallas_call(state_kernel, grid=(own,), out_shape=[jax.ShapeDtypeStruct...  15.2 us
    unnamed x29, local copies, waits for them, and re-layouts  11.4 us

profile of v1, /device:TPU:0, one launch (start us, length us, event | category | flops | bytes accessed | tf_op | source)
XLA Modules:
  0.0 112.8 jit_solution(16570014084378240122)
XLA Ops:
  0.6 0.0 copy-start.7
  0.6 0.0 copy-start.13
  0.7 0.7 convert_element_type.3
  1.3 0.1 fusion
  1.5 0.1 pad_maximum_fusion
  1.5 0.0 copy-start.1
  1.5 1.2 %copy-done.1 = bf16[512,1024]{1,0:T(8,128)(2,1)S(1)} copy-done((bf16[512,1024]{1,0:T(8,128)(2,1)S(1)}, bf16[512,1024]{1,0:T(8,128)(2,1)}, u32[]{:S(2)}) %copy-start.1) | copy-done | bytes 1048600
  2.8 0.0 copy-start.2
  2.8 1.2 %copy-done.2 = bf16[512,1024]{1,0:T(8,128)(2,1)S(1)} copy-done((bf16[512,1024]{1,0:T(8,128)(2,1)S(1)}, bf16[512,1024]{1,0:T(8,128)(2,1)}, u32[]{:S(2)}) %copy-start.2) | copy-done | bytes 1048600
  4.0 0.0 copy-start.4
  4.0 1.0 copy-done.4
  5.0 0.0 copy-start.5
  5.0 1.0 copy-done.5
  6.1 0.0 copy-start.6
  6.1 0.8 copy-done.6
  6.8 0.0 copy-start.12
  6.8 0.7 copy-done.12
  7.5 0.0 copy-start.3
  7.5 25.2 %shard_map.140 = (f32[16,8,128]{2,1,0:T(8,128)S(1)}, f32[16,4,256]{2,1,0:T(4,128)S(1)}, f32[16,4,256]{2,1,0:T(4,128)S(1)}) custom-call(bf16[32,512]{1,0:T(8,128)(2,1)S(1)} %copy-done.6, f32[1,512]{1,0:T(1,128)S(1)} %bitcast.3, f32[16,128]{1,0:T(8,128)S(1)} %get-tuple-element.15.cosine, f32[16,128]{1,0:T(8,128)S(1)} %get-tuple-element.16.sine, ...), custom_call_target="tpu_custom_call" | custom-call | tf_op jit(solution)/shard_map/pallas_call | solution.py:378
  32.7 0.0 copy-start.8
  32.7 0.6 copy-done.8
  33.3 0.6 copy-done.9
  34.0 0.6 copy-done.10
  34.6 15.2 %shard_map.141 = (f32[16,4,128,256]{3,2,1,0:T(8,128)}, bf16[16,1024]{1,0:T(8,128)(2,1)}) custom-call(f32[16,8,128]{2,1,0:T(8,128)} %copy-done.8, f32[16,4,256]{2,1,0:T(4,128)} %copy-done.9, f32[16,4,256]{2,1,0:T(4,128)} %copy-done.10, f32[1,1024]{1,0:T(1,128)} %bitcast.5, f32[16,4,128,256]{3,2,1,0:T(8,128)} %state.1), custom_call_target="tpu_custom_call" | custom-call | tf_op jit(solution)/shard_map/pallas_call | solution.py:402
  49.8 0.0 copy-done.7
  49.8 0.0 copy-done.13
  49.8 0.0 copy-done.3
  49.8 0.0 copy-start
  49.8 2.2 %copy-done = bf16[512,4096]{1,0:T(8,128)(2,1)S(1)} copy-done((bf16[512,4096]{1,0:T(8,128)(2,1)S(1)}, bf16[512,4096]{1,0:T(8,128)(2,1)}, u32[]{:S(2)}) %copy-start) | copy-done | bytes 4194328
  52.0 0.8 copy-done.11
  52.8 59.5 %shard_map.142 = bf16[32,512]{1,0:T(8,128)(2,1)S(1)} custom-call(bf16[16,1024]{1,0:T(8,128)(2,1)S(1)} %copy-done.11, bf16[32,512]{1,0:T(8,128)(2,1)S(1)} %copy-done.7, f32[1,512]{1,0:T(1,128)S(1)} %bitcast.4, bf16[1024,512]{1,0:T(8,128)(2,1)S(1)} %copy-done.3, bf16[512,4096]{1,0:T(8,128)(2,1)S(1)} %copy-done, bf16[4096,512]{1,0:T(8,128)(2,1)} %w_down.1), custom_call_target="tpu_custom_call" | custom-call | tf_op jit(solution)/shard_map/pallas_call | solution.py:422
  112.2 0.6 copy.16
  (4 shorter events, 0.0 us)
Async XLA Ops:
  0.6 49.2 %copy-start.7 = (bf16[32,512]{1,0:T(8,128)(2,1)S(1)}, bf16[32,512]{1,0:T(8,128)(2,1)}, u32[]{:S(2)}) copy-start(bf16[32,512]{1,0:T(8,128)(2,1)} %tokens.3) | copy-start | bytes 98308
  0.6 49.2 %copy-start.13 = (f32[512]{0:T(512)S(1)}, f32[512]{0:T(512)}, u32[]{:S(2)}) copy-start(f32[512]{0:T(512)} %param.23) | copy-start | bytes 6148
  1.5 1.2 %copy-start.1 = (bf16[512,1024]{1,0:T(8,128)(2,1)S(1)}, bf16[512,1024]{1,0:T(8,128)(2,1)}, u32[]{:S(2)}) copy-start(bf16[512,1024]{1,0:T(8,128)(2,1)} %wv.1) | copy-start | bytes 3145732
  2.8 1.2 %copy-start.2 = (bf16[512,1024]{1,0:T(8,128)(2,1)S(1)}, bf16[512,1024]{1,0:T(8,128)(2,1)}, u32[]{:S(2)}) copy-start(bf16[512,1024]{1,0:T(8,128)(2,1)} %wg.1) | copy-start | bytes 3145732
  4.0 1.0 copy-start.4
  5.0 1.0 copy-start.5
  6.1 0.8 copy-start.6
  6.8 0.7 copy-start.12
  7.5 42.3 %copy-start.3 = (bf16[1024,512]{1,0:T(8,128)(2,1)S(1)}, bf16[1024,512]{1,0:T(8,128)(2,1)}, u32[]{:S(2)}) copy-start(bf16[1024,512]{1,0:T(8,128)(2,1)} %w_out.1) | copy-start | bytes 3145732
  32.7 0.6 copy-start.8
  33.3 0.6 copy-start.9
  34.0 0.6 copy-start.10
  49.8 2.2 %copy-start = (bf16[512,4096]{1,0:T(8,128)(2,1)S(1)}, bf16[512,4096]{1,0:T(8,128)(2,1)}, u32[]{:S(2)}) copy-start(bf16[512,4096]{1,0:T(8,128)(2,1)} %w_hidden.1) | copy-start | bytes 12582916
  52.0 0.8 copy-start.11

commit v2 on v1

--- a/solution.py
+++ b/solution.py
@@ -187,15 +187,36 @@
         return list(self.first.values()) + list(self.second.values())
 
 
-def project_kernel(
-    n_kv, n_tp, inner, features,
-    tokens, gain, cosine, sine, wq, wk, wv, wg,
-    qk_out, v_out, g_out,
-    rows, weights, terms, land_in, partial, land_out, squares, squares_in,
-    w_sem, tp_send, tp_recv, sq_send, sq_recv, s1, r1, s2, r2,
+def layer_kernel(
+    n_kv, n_tp, inner, features, wide,
+    cosine, sine, tokens_hbm, gain_hbm, mid_gain_hbm, head_gain_hbm,
+    wq, wk, wv, wg, w_out, w_hidden, w_down, state,
+    output, new_state,
+    tokens, gain, mid_gain, head_gain,
+    rows, weights, terms, land_in, partial, land_out, squares, squares_in, qk, values, gates, mixed,
+    held, wo, wh, wd, out_terms, out_land, resid, rows_mid, squares_mid, squares_mid_in,
+    terms_h, land_in_h, partial_h, land_out_h, active, acc, down_terms, down_land,
+    small_sem, w_sem, state_sem,
+    tp_send, tp_recv, sq_send, sq_recv, s1, r1, s2, r2,
+    gs1, gr1, gs2, gr2, os, orr, ts, tr, qs, qr, hs1, hr1, hs2, hr2, as1, ar1, as2, ar2, ds, dr,
 ):
     outer = n_kv // inner
     own = cosine.shape[0]
+    me = lax.axis_index("kv")
+    o, i = me // inner, lax.rem(me, inner)
+    small = [
+        pltpu.make_async_copy(src, dst, small_sem.at[at])
+        for at, (src, dst) in enumerate(
+            (
+                (tokens_hbm, tokens),
+                (gain_hbm, gain),
+                (mid_gain_hbm, mid_gain),
+                (head_gain_hbm, head_gain),
+            )
+        )
+    ]
+    for load in small:
+        load.start()
     loads, offset = [], 0
     for index, ref in enumerate((wq, wk, wv, wg)):
         width = ref.shape[1]
@@ -204,10 +225,19 @@
         offset += width
     for load, _, _ in loads:
         load.start()
+    late = [
+        pltpu.make_async_copy(w_out, wo, w_sem.at[4]),
+        pltpu.make_async_copy(w_hidden, wh, w_sem.at[5]),
+        pltpu.make_async_copy(w_down, wd, w_sem.at[6]),
+    ]
+    state_load = pltpu.make_async_copy(state, new_state, state_sem.at[0])
     entry_barrier(n_kv, n_tp)
+    for load in small:
+        load.wait()
     pending = gather_tp(tokens, rows, tp_send, tp_recv, n_tp)
     batch = rows.shape[0] * rows.shape[1]
-    x = rows[...].reshape(batch, rows.shape[2]).astype(jnp.float32)
+    piece, cols = tokens.shape
+    x = rows[...].reshape(batch, cols).astype(jnp.float32)
     total = jnp.sum(x * x, axis=1, keepdims=True)
     squares[...] = jnp.broadcast_to(total, (batch, 128)).reshape(n_kv, own, 128)
     sq_copies = squares_start(squares, squares_in, sq_send, sq_recv, n_kv)
@@ -220,6 +250,9 @@
         terms[:, :, :, offset : offset + width] = term.reshape(outer, inner, own, width)
     scatter = Scatter(terms, land_in, partial, land_out, (s1, r1, s2, r2), outer, inner)
     scatter.start()
+    state_load.start()
+    for load in late:
+        load.start()
     scatter.middle()
     scale = lax.rsqrt(squares_total(sq_copies, squares, squares_in) / features + EPS)
     scatter.arrived()
@@ -230,103 +263,76 @@
         turned = vec * c + pltpu.roll(vec, DK // 2, 1) * s
         if h >= heads:
             turned = turned * DK ** (-0.5)
-        qk_out[:, h, :] = turned
+        qk[:, h, :] = turned
     for h in range(heads):
-        v_out[:, h, :] = scatter.total(pl.ds(2 * heads * DK + h * DV, DV)) * scale
-        g_out[:, h, :] = scatter.total(pl.ds(heads * (2 * DK + DV) + h * DV, DV)) * scale
-    for copy in pending + sq_copies + scatter.copies():
-        copy.wait_send()
-
-
-def state_kernel(qk, v, g, gain, state, new_state, mixed, acc):
-    heads = state.shape[1]
-    b = pl.program_id(0)
-    columns = qk[0].T
+        values[:, h, :] = scatter.total(pl.ds(2 * heads * DK + h * DV, DV)) * scale
+        gates[:, h, :] = scatter.total(pl.ds(heads * (2 * DK + DV) + h * DV, DV)) * scale
+    pending += sq_copies + scatter.copies()
     first = lax.axis_index("tp") * heads
-    for h in range(heads):
-        ids = jnp.full((1, DV), first + h, jnp.int32).astype(jnp.float32)
-        decay = 1.0 - jnp.exp2(-2.0 - 6.0 * ids / (H - 1))
-        query = columns[:, h : h + 1]
-        key = columns[:, heads + h : heads + h + 1]
-        new = decay * state[0, h] + key * v[0, h : h + 1, :]
-        new_state[0, h] = new
-        read = jnp.sum(query * new, axis=0, keepdims=True)
-        read = read * lax.rsqrt(jnp.mean(read * read, axis=-1, keepdims=True) + EPS)
-        gate = g[0, h : h + 1, :]
-        part = slice(h * DV, (h + 1) * DV)
-        acc[pl.ds(b, 1), part] = read * gain[:, part] * (gate / (1.0 + jnp.exp(-gate)))
-
-    @pl.when(b == pl.num_programs(0) - 1)
-    def _():
-        mixed[...] = acc[...].astype(jnp.bfloat16)
-
-
-def mixer_kernel(
-    n_kv, n_tp, inner, features, wide,
-    mixed, tokens, gain, w_out, w_hidden, w_down,
-    output,
-    held, wo, wh, wd, out_terms, out_land, resid, rows, squares, squares_in,
-    terms, land_in, partial, land_out, active, acc, down_terms, down_land,
-    w_sem, gs1, gr1, gs2, gr2, os, orr, ts, tr, qs, qr, s1, r1, s2, r2, hs1, hr1, hs2, hr2, ds, dr,
-):
-    outer = n_kv // inner
-    own, width = mixed.shape
-    me = lax.axis_index("kv")
-    loads = [
-        pltpu.make_async_copy(w_out, wo, w_sem.at[0]),
-        pltpu.make_async_copy(w_hidden, wh, w_sem.at[1]),
-        pltpu.make_async_copy(w_down, wd, w_sem.at[2]),
-    ]
-    for load in loads:
-        load.start()
-    o, i = me // inner, lax.rem(me, inner)
-    held[o, i] = mixed[...]
-    entry_barrier(n_kv, n_tp)
+    state_load.wait()
+
+    @pl.loop(0, own)
+    def _(b):
+        columns = qk[b].T
+        v, g = values[b], gates[b]
+        for h in range(heads):
+            ids = jnp.full((1, DV), first + h, jnp.int32).astype(jnp.float32)
+            decay = 1.0 - jnp.exp2(-2.0 - 6.0 * ids / (heads * n_tp - 1))
+            query = columns[:, h : h + 1]
+            key = columns[:, heads + h : heads + h + 1]
+            new = decay * new_state[b, h] + key * v[h : h + 1, :]
+            new_state[b, h] = new
+            read = jnp.sum(query * new, axis=0, keepdims=True)
+            read = read * lax.rsqrt(jnp.mean(read * read, axis=-1, keepdims=True) + EPS)
+            gate = g[h : h + 1, :]
+            part = slice(h * DV, (h + 1) * DV)
+            mixed[pl.ds(b, 1), part] = read * head_gain[:, part] * (gate / (1.0 + jnp.exp(-gate)))
+
+    held[o, i] = mixed[...].astype(jnp.bfloat16)
     gather = Gather(held, (gs1, gr1, gs2, gr2), outer, inner)
     gather.run()
-    pending = gather.copies()
-    loads[0].wait()
-    batch = n_kv * own
-    piece = batch // n_tp
-    cols = wo.shape[1]
+    pending += gather.copies()
+    late[0].wait()
     out_terms[...] = (
-        jnp.dot(held[...].reshape(batch, width), wo[...], preferred_element_type=jnp.float32)
+        jnp.dot(
+            held[...].reshape(batch, mixed.shape[1]), wo[...], preferred_element_type=jnp.float32
+        )
         .astype(jnp.bfloat16)
         .reshape(n_tp, piece, cols)
     )
     attn, copies = reduce_tp(out_terms, out_land, os, orr, n_tp)
     pending += copies
     resid[...] = (tokens[...].astype(jnp.float32) + attn).astype(jnp.bfloat16)
-    pending += gather_tp(resid, rows, ts, tr, n_tp)
-    x = rows[...].reshape(batch, cols).astype(jnp.float32)
+    pending += gather_tp(resid, rows_mid, ts, tr, n_tp)
+    x = rows_mid[...].reshape(batch, cols).astype(jnp.float32)
     total = jnp.sum(x * x, axis=1, keepdims=True)
-    squares[...] = jnp.broadcast_to(total, (batch, 128)).reshape(n_kv, own, 128)
-    sq_copies = squares_start(squares, squares_in, qs, qr, n_kv)
+    squares_mid[...] = jnp.broadcast_to(total, (batch, 128)).reshape(n_kv, own, 128)
+    sq_copies = squares_start(squares_mid, squares_mid_in, qs, qr, n_kv)
     pending += sq_copies
-    normed = (x * gain[...]).astype(jnp.bfloat16)
-    loads[1].wait()
+    normed = (x * mid_gain[...]).astype(jnp.bfloat16)
+    late[1].wait()
     hidden = wh.shape[1]
 
     @pl.loop(0, hidden // wide)
     def _(c):
         part = pl.ds(pl.multiple_of(c * wide, wide), wide)
         term = jnp.dot(normed, wh[:, part], preferred_element_type=jnp.float32)
-        terms[:, :, :, part] = term.astype(jnp.bfloat16).reshape(outer, inner, own, wide)
-
-    scatter = Scatter(terms, land_in, partial, land_out, (s1, r1, s2, r2), outer, inner)
+        terms_h[:, :, :, part] = term.astype(jnp.bfloat16).reshape(outer, inner, own, wide)
+
+    scatter = Scatter(terms_h, land_in_h, partial_h, land_out_h, (hs1, hr1, hs2, hr2), outer, inner)
     scatter.start()
     scatter.middle()
-    scale = lax.rsqrt(squares_total(sq_copies, squares, squares_in) / features + EPS)
+    scale = lax.rsqrt(squares_total(sq_copies, squares_mid, squares_mid_in) / features + EPS)
     scatter.arrived()
     pending += scatter.copies()
     for c in range(hidden // wide):
         part = pl.ds(c * wide, wide)
         value = jnp.maximum(scatter.total(part) * scale, 0.0)
         active[o, i, :, part] = (value * value).astype(jnp.bfloat16)
-    gather = Gather(active, (hs1, hr1, hs2, hr2), outer, inner)
+    gather = Gather(active, (as1, ar1, as2, ar2), outer, inner)
     gather.run()
     pending += gather.copies()
-    loads[2].wait()
+    late[2].wait()
     acc[...] = jnp.zeros_like(acc)
 
     @pl.loop(0, hidden // wide)
@@ -361,7 +367,9 @@
     piece, cols = tokens.shape
     heads = state.shape[1]
     whole = heads * 2 * (DK + DV)
-    vmem, hbm = pl.BlockSpec(memory_space=VMEM), pl.BlockSpec(memory_space=pl.ANY)
+    hidden = hidden_weight.shape[1]
+    wide = min(512, hidden)
+    vmem, hbm = pl.BlockSpec(memory_space=VMEM), pl.BlockSpec(memory_space=pltpu.HBM)
 
     def scatter_buffers(width):
         return [
@@ -375,85 +383,56 @@
     two_out = [DMA((outer,)), DMA((outer,))]
     over_tp = [DMA((n_tp,)), DMA((n_tp,))]
     over_kv = [DMA((n_kv,)), DMA((n_kv,))]
-    qk, v, g = pl.pallas_call(
-        functools.partial(project_kernel, n_kv, n_tp, inner, features),
+    squares = [VMEM((n_kv, own, 128), f32), VMEM((n_kv, own, 128), f32)]
+    tp_rows = VMEM((n_tp, piece, cols), bf16)
+    return pl.pallas_call(
+        functools.partial(layer_kernel, n_kv, n_tp, inner, features, wide),
         out_shape=[
-            jax.ShapeDtypeStruct((own, 2 * heads, DK), f32),
-            jax.ShapeDtypeStruct((own, heads, DV), f32),
-            jax.ShapeDtypeStruct((own, heads, DV), f32),
+            jax.ShapeDtypeStruct(tokens.shape, bf16),
+            jax.ShapeDtypeStruct(state.shape, f32),
         ],
-        in_specs=[vmem] * 4 + [hbm] * 4,
-        out_specs=[vmem] * 3,
-        scratch_shapes=[VMEM((n_tp, piece, cols), bf16), VMEM((cols, whole), bf16)]
+        in_specs=[vmem] * 2 + [hbm] * 12,
+        out_specs=[vmem] * 2,
+        scratch_shapes=[
+            VMEM(tokens.shape, bf16), VMEM((1, cols), f32), VMEM((1, cols), f32),
+            VMEM((1, heads * DV), f32),
+            tp_rows, VMEM((cols, whole), bf16),
+        ]
         + scatter_buffers(whole)
-        + [VMEM((n_kv, own, 128), f32), VMEM((n_kv, own, 128), f32), DMA((4,))]
-        + over_tp + over_kv + two_in + two_out,
-        compiler_params=pltpu.CompilerParams(
-            collective_id=0, has_side_effects=True, vmem_limit_bytes=48 * 2**20
-        ),
-    )(
-        tokens, norm_in_gain[None, :], cosine, sine,
-        query_weight, key_weight, value_weight, gate_weight,
-    )
-
-    def per_row(*shape):
-        return pl.BlockSpec((1,) + shape, lambda b: (b,) + (0,) * len(shape))
-
-    new_state, mixed = pl.pallas_call(
-        state_kernel,
-        grid=(own,),
-        out_shape=[
-            jax.ShapeDtypeStruct(state.shape, f32),
-            jax.ShapeDtypeStruct((own, heads * DV), bf16),
-        ],
-        in_specs=[
-            per_row(2 * heads, DK),
-            per_row(heads, DV),
-            per_row(heads, DV),
-            pl.BlockSpec((1, heads * DV), lambda b: (0, 0)),
-            per_row(heads, DK, DV),
-        ],
-        out_specs=[per_row(heads, DK, DV), pl.BlockSpec((own, heads * DV), lambda b: (0, 0))],
-        scratch_shapes=[VMEM((own, heads * DV), f32)],
-    )(qk, v, g, head_gain[None, :], state)
-
-    hidden = hidden_weight.shape[1]
-    wide = min(512, hidden)
-    output = pl.pallas_call(
-        functools.partial(mixer_kernel, n_kv, n_tp, inner, features, wide),
-        out_shape=jax.ShapeDtypeStruct(tokens.shape, bf16),
-        in_specs=[vmem] * 3 + [hbm] * 3,
-        out_specs=vmem,
-        scratch_shapes=[
+        + squares
+        + [
+            VMEM((own, 2 * heads, DK), f32),
+            VMEM((own, heads, DV), f32),
+            VMEM((own, heads, DV), f32),
+            VMEM((own, heads * DV), f32),
             VMEM((outer, inner, own, heads * DV), bf16),
             VMEM(out_weight.shape, bf16),
             VMEM(hidden_weight.shape, bf16),
             VMEM(down_weight.shape, bf16),
-            VMEM((n_tp, piece, cols), bf16),
-            VMEM((n_tp, piece, cols), bf16),
-            VMEM((piece, cols), bf16),
-            VMEM((n_tp, piece, cols), bf16),
-            VMEM((n_kv, own, 128), f32),
-            VMEM((n_kv, own, 128), f32),
+            tp_rows, tp_rows, VMEM((piece, cols), bf16), tp_rows,
         ]
+        + squares
         + scatter_buffers(hidden)
         + [
             VMEM((outer, inner, own, hidden), bf16),
             VMEM((n_tp * piece, cols), f32),
-            VMEM((n_tp, piece, cols), bf16),
-            VMEM((n_tp, piece, cols), bf16),
-            DMA((3,)),
+            tp_rows, tp_rows,
+            DMA((4,)), DMA((7,)), DMA((1,)),
         ]
+        + over_tp + over_kv + two_in + two_out
         + two_out + two_in
         + over_tp + over_tp + over_kv
         + two_in + two_out
         + two_out + two_in
         + over_tp,
         compiler_params=pltpu.CompilerParams(
-            collective_id=1, has_side_effects=True, vmem_limit_bytes=48 * 2**20
+            collective_id=0, has_side_effects=True, vmem_limit_bytes=48 * 2**20
         ),
-    )(mixed, tokens, norm_mlp_gain[None, :], out_weight, hidden_weight, down_weight)
-    return output, new_state
+    )(
+        cosine, sine, tokens, norm_in_gain[None, :], norm_mlp_gain[None, :], head_gain[None, :],
+        query_weight, key_weight, value_weight, gate_weight,
+        out_weight, hidden_weight, down_weight, state,
+    )
 
 
 def inner_size(mesh):

time: 115 us -> 114 us (level)
  Pallas kernels: 99.9 us -> 93.6 us
  local copies, waits for them, and re-layouts: 11.4 us -> 17 us
    pallas_call x3 -> x1, Pallas kernels: 99.9 us -> 93.6 us  [local(): pl.pallas_call(functools.partial(layer_kernel, n_kv, n_tp, inner, feature...]
    unnamed x29 -> x20, local copies, waits for them, and re-layouts: 11.4 us -> 17 us
where the time goes in v2:
time: 114 us; the launch traced here: 112 us
  Pallas kernels  93.6 us (82%)
  local copies, waits for them, and re-layouts  17 us (15%)
    pallas_call x1, Pallas kernels, local(): pl.pallas_call(functools.partial(layer_kernel, n_kv, n_tp, inner, feature...  93.6 us
    unnamed x20, local copies, waits for them, and re-layouts  17 us

profile of v2, /device:TPU:0, one launch (start us, length us, event | category | flops | bytes accessed | tf_op | source)
XLA Modules:
  0.0 112.1 jit_solution(11957197834287515311)
XLA Ops:
  0.6 0.7 convert_element_type.3
  1.3 0.1 fusion
  1.4 0.1 pad_maximum_fusion
  1.5 0.0 copy-start
  1.5 1.2 %copy-done = bf16[512,1024]{1,0:T(8,128)(2,1)S(1)} copy-done((bf16[512,1024]{1,0:T(8,128)(2,1)S(1)}, bf16[512,1024]{1,0:T(8,128)(2,1)}, u32[]{:S(2)}) %copy-start) | copy-done | bytes 1048600
  2.7 0.0 copy-start.1
  2.7 1.2 %copy-done.1 = bf16[512,1024]{1,0:T(8,128)(2,1)S(1)} copy-done((bf16[512,1024]{1,0:T(8,128)(2,1)S(1)}, bf16[512,1024]{1,0:T(8,128)(2,1)}, u32[]{:S(2)}) %copy-start.1) | copy-done | bytes 1048600
  4.0 0.0 copy-start.2
  4.0 1.2 %copy-done.2 = bf16[1024,512]{1,0:T(8,128)(2,1)S(1)} copy-done((bf16[1024,512]{1,0:T(8,128)(2,1)S(1)}, bf16[1024,512]{1,0:T(8,128)(2,1)}, u32[]{:S(2)}) %copy-start.2) | copy-done | bytes 1048600
  5.2 0.0 copy-start.3
  5.2 1.0 copy-done.3
  6.2 0.0 copy-start.4
  6.2 1.0 copy-done.4
  7.3 0.0 copy-start.5
  7.3 0.8 copy-done.5
  8.0 0.0 copy-start.6
  8.0 0.7 copy-done.6
  8.7 0.0 copy-start.7
  8.7 0.7 copy-done.7
  9.4 0.0 copy-start.8
  9.4 0.7 copy-done.8
  10.1 93.6 %shard_map.140 = (bf16[32,512]{1,0:T(8,128)(2,1)S(1)}, f32[16,4,128,256]{3,2,1,0:T(8,128)}) custom-call(f32[16,128]{1,0:T(8,128)S(1)} %get-tuple-element.5.cosine, f32[16,128]{1,0:T(8,128)S(1)} %get-tuple-element.6.sine, bf16[32,512]{1,0:T(8,128)(2,1)S(1)} %copy-done.5, f32[1,512]{1,0:T(1,128)S(1)} %bitcast.4, f32[1,512]{1,0:T(1,128)S(1)} %bitcast.5, ...), custom_call_target="tpu_custom_call" | custom-call | tf_op jit(solution)/shard_map/pallas_call | solution.py:388
  103.7 0.6 copy.17
  104.3 7.8 %copy.18 = f32[16,4,128,256]{3,2,1,0:T(8,128)} copy(f32[16,4,128,256]{3,2,1,0:T(8,128)} %get-tuple-element.10) | data formatting | bytes 16777216
  (1 shorter events, 0.0 us)
Async XLA Ops:
  1.5 1.2 %copy-start = (bf16[512,1024]{1,0:T(8,128)(2,1)S(1)}, bf16[512,1024]{1,0:T(8,128)(2,1)}, u32[]{:S(2)}) copy-start(bf16[512,1024]{1,0:T(8,128)(2,1)} %wv.1) | copy-start | bytes 3145732
  2.7 1.2 %copy-start.1 = (bf16[512,1024]{1,0:T(8,128)(2,1)S(1)}, bf16[512,1024]{1,0:T(8,128)(2,1)}, u32[]{:S(2)}) copy-start(bf16[512,1024]{1,0:T(8,128)(2,1)} %wg.1) | copy-start | bytes 3145732
  4.0 1.2 %copy-start.2 = (bf16[1024,512]{1,0:T(8,128)(2,1)S(1)}, bf16[1024,512]{1,0:T(8,128)(2,1)}, u32[]{:S(2)}) copy-start(bf16[1024,512]{1,0:T(8,128)(2,1)} %w_out.1) | copy-start | bytes 3145732
  5.2 1.0 copy-start.3
  6.2 1.0 copy-start.4
  7.3 0.8 copy-start.5
  8.0 0.7 copy-start.6
  8.7 0.7 copy-start.7
  9.4 0.7 copy-start.8

commit v3 on v2

--- a/solution.py
+++ b/solution.py
@@ -11,6 +11,7 @@
 DK = 128
 DV = 256
 EPS = 1e-06
+CHUNKS = 2
 MESH = pl.DeviceIdType.MESH
 VMEM = pltpu.VMEM
 DMA = pltpu.SemaphoreType.DMA
@@ -172,14 +173,18 @@
                     {"kv": o * inner + lax.rem(i + k, inner)},
                 )
 
-    def run(self):
+    def start(self):
         for copy in self.first.values():
             copy.start()
+
+    def forward(self):
         for s in range(self.outer):
             if s:
                 self.first[s].wait_recv()
             for k in range(1, self.inner):
                 self.second[s, k].start()
+
+    def arrived(self):
         for copy in self.second.values():
             copy.wait_recv()
 
@@ -193,11 +198,12 @@
     wq, wk, wv, wg, w_out, w_hidden, w_down, state,
     output, new_state,
     tokens, gain, mid_gain, head_gain,
-    rows, weights, terms, land_in, partial, land_out, squares, squares_in, qk, values, gates, mixed,
+    rows, weights, terms, land_in, partial, land_out, g_terms, g_land_in, g_partial, g_land_out,
+    squares, squares_in, qk, values, mixed, held_state, fresh, columns,
     held, wo, wh, wd, out_terms, out_land, resid, rows_mid, squares_mid, squares_mid_in,
     terms_h, land_in_h, partial_h, land_out_h, active, acc, down_terms, down_land,
     small_sem, w_sem, state_sem,
-    tp_send, tp_recv, sq_send, sq_recv, s1, r1, s2, r2,
+    tp_send, tp_recv, sq_send, sq_recv, s1, r1, s2, r2, t1, u1, t2, u2,
     gs1, gr1, gs2, gr2, os, orr, ts, tr, qs, qr, hs1, hr1, hs2, hr2, as1, ar1, as2, ar2, ds, dr,
 ):
     outer = n_kv // inner
@@ -230,7 +236,7 @@
         pltpu.make_async_copy(w_hidden, wh, w_sem.at[5]),
         pltpu.make_async_copy(w_down, wd, w_sem.at[6]),
     ]
-    state_load = pltpu.make_async_copy(state, new_state, state_sem.at[0])
+    state_load = pltpu.make_async_copy(state, held_state, state_sem.at[0])
     entry_barrier(n_kv, n_tp)
     for load in small:
         load.wait()
@@ -242,18 +248,25 @@
     squares[...] = jnp.broadcast_to(total, (batch, 128)).reshape(n_kv, own, 128)
     sq_copies = squares_start(squares, squares_in, sq_send, sq_recv, n_kv)
     normed = (x * gain[...]).astype(jnp.bfloat16)
-    for load, offset, width in loads:
+    scatter = Scatter(terms, land_in, partial, land_out, (s1, r1, s2, r2), outer, inner)
+    gating = Scatter(g_terms, g_land_in, g_partial, g_land_out, (t1, u1, t2, u2), outer, inner)
+    for index, (load, offset, width) in enumerate(loads):
         load.wait()
         term = jnp.dot(
             normed, weights[:, offset : offset + width], preferred_element_type=jnp.float32
         ).astype(jnp.bfloat16)
-        terms[:, :, :, offset : offset + width] = term.reshape(outer, inner, own, width)
-    scatter = Scatter(terms, land_in, partial, land_out, (s1, r1, s2, r2), outer, inner)
-    scatter.start()
+        if index < 3:
+            terms[:, :, :, offset : offset + width] = term.reshape(outer, inner, own, width)
+        else:
+            g_terms[...] = term.reshape(outer, inner, own, width)
+        if index == 2:
+            scatter.start()
+    gating.start()
     state_load.start()
     for load in late:
         load.start()
     scatter.middle()
+    gating.middle()
     scale = lax.rsqrt(squares_total(sq_copies, squares, squares_in) / features + EPS)
     scatter.arrived()
     c, s = cosine[...], sine[...]
@@ -266,31 +279,40 @@
         qk[:, h, :] = turned
     for h in range(heads):
         values[:, h, :] = scatter.total(pl.ds(2 * heads * DK + h * DV, DV)) * scale
-        gates[:, h, :] = scatter.total(pl.ds(heads * (2 * DK + DV) + h * DV, DV)) * scale
-    pending += sq_copies + scatter.copies()
+    pending += sq_copies + scatter.copies() + gating.copies()
     first = lax.axis_index("tp") * heads
     state_load.wait()
 
-    @pl.loop(0, own)
+    decays = []
+    for h in range(heads):
+        ids = jnp.full((1, DV), first + h, jnp.int32).astype(jnp.float32)
+        decays.append(1.0 - jnp.exp2(-2.0 - 6.0 * ids / (heads * n_tp - 1)))
+    for b in range(own):
+        columns[b] = qk[b].T
+
+    @pl.loop(0, own, unroll=2)
     def _(b):
-        columns = qk[b].T
-        v, g = values[b], gates[b]
         for h in range(heads):
-            ids = jnp.full((1, DV), first + h, jnp.int32).astype(jnp.float32)
-            decay = 1.0 - jnp.exp2(-2.0 - 6.0 * ids / (heads * n_tp - 1))
-            query = columns[:, h : h + 1]
-            key = columns[:, heads + h : heads + h + 1]
-            new = decay * new_state[b, h] + key * v[h : h + 1, :]
-            new_state[b, h] = new
-            read = jnp.sum(query * new, axis=0, keepdims=True)
-            read = read * lax.rsqrt(jnp.mean(read * read, axis=-1, keepdims=True) + EPS)
-            gate = g[h : h + 1, :]
-            part = slice(h * DV, (h + 1) * DV)
-            mixed[pl.ds(b, 1), part] = read * head_gain[:, part] * (gate / (1.0 + jnp.exp(-gate)))
-
-    held[o, i] = mixed[...].astype(jnp.bfloat16)
+            query = columns[b, :, h : h + 1]
+            key = columns[b, :, heads + h : heads + h + 1]
+            new = decays[h] * held_state[b, h] + key * values[b, h : h + 1, :]
+            fresh[b, h] = new
+            mixed[pl.ds(b, 1), h * DV : (h + 1) * DV] = jnp.sum(query * new, axis=0, keepdims=True)
+
+    state_store = pltpu.make_async_copy(fresh, new_state, state_sem.at[1])
+    state_store.start()
+    gating.arrived()
+    for h in range(heads):
+        part = pl.ds(h * DV, DV)
+        gate = gating.total(part) * scale
+        read = mixed[:, part]
+        read = read * lax.rsqrt(jnp.mean(read * read, axis=-1, keepdims=True) + EPS)
+        value = read * head_gain[:, part] * (gate / (1.0 + jnp.exp(-gate)))
+        held[o, i, :, part] = value.astype(jnp.bfloat16)
     gather = Gather(held, (gs1, gr1, gs2, gr2), outer, inner)
-    gather.run()
+    gather.start()
+    gather.forward()
+    gather.arrived()
     pending += gather.copies()
     late[0].wait()
     out_terms[...] = (
@@ -313,38 +335,60 @@
     late[1].wait()
     hidden = wh.shape[1]
 
-    @pl.loop(0, hidden // wide)
-    def _(c):
-        part = pl.ds(pl.multiple_of(c * wide, wide), wide)
-        term = jnp.dot(normed, wh[:, part], preferred_element_type=jnp.float32)
-        terms_h[:, :, :, part] = term.astype(jnp.bfloat16).reshape(outer, inner, own, wide)
-
-    scatter = Scatter(terms_h, land_in_h, partial_h, land_out_h, (hs1, hr1, hs2, hr2), outer, inner)
-    scatter.start()
-    scatter.middle()
+    steps = hidden // CHUNKS // wide
+    scatters, gathers = [], []
+    for chunk in range(CHUNKS):
+
+        @pl.loop(0, steps)
+        def _(c):
+            here = pl.ds(pl.multiple_of((chunk * steps + c) * wide, wide), wide)
+            part = pl.ds(pl.multiple_of(c * wide, wide), wide)
+            term = jnp.dot(normed, wh[:, here], preferred_element_type=jnp.float32)
+            terms_h[chunk, :, :, :, part] = term.astype(jnp.bfloat16).reshape(
+                outer, inner, own, wide
+            )
+
+        scatter = Scatter(
+            terms_h.at[chunk], land_in_h.at[chunk], partial_h.at[chunk], land_out_h.at[chunk],
+            [sem.at[chunk] for sem in (hs1, hr1, hs2, hr2)], outer, inner,
+        )
+        scatter.start()
+        scatters.append(scatter)
+    for scatter in scatters:
+        scatter.middle()
     scale = lax.rsqrt(squares_total(sq_copies, squares_mid, squares_mid_in) / features + EPS)
-    scatter.arrived()
-    pending += scatter.copies()
-    for c in range(hidden // wide):
-        part = pl.ds(c * wide, wide)
-        value = jnp.maximum(scatter.total(part) * scale, 0.0)
-        active[o, i, :, part] = (value * value).astype(jnp.bfloat16)
-    gather = Gather(active, (as1, ar1, as2, ar2), outer, inner)
-    gather.run()
-    pending += gather.copies()
+    for chunk, scatter in enumerate(scatters):
+        scatter.arrived()
+        pending += scatter.copies()
+        for c in range(steps):
+            part = pl.ds(c * wide, wide)
+            value = jnp.maximum(scatter.total(part) * scale, 0.0)
+            active[chunk, o, i, :, part] = (value * value).astype(jnp.bfloat16)
+        gather = Gather(
+            active.at[chunk], [sem.at[chunk] for sem in (as1, ar1, as2, ar2)], outer, inner
+        )
+        gather.start()
+        gathers.append(gather)
+    for gather in gathers:
+        gather.forward()
     late[2].wait()
     acc[...] = jnp.zeros_like(acc)
-
-    @pl.loop(0, hidden // wide)
-    def _(c):
-        part = pl.ds(pl.multiple_of(c * wide, wide), wide)
-        left = active[:, :, :, part].reshape(batch, wide)
-        acc[...] += jnp.dot(left, wd[part, :], preferred_element_type=jnp.float32)
+    for chunk, gather in enumerate(gathers):
+        gather.arrived()
+        pending += gather.copies()
+
+        @pl.loop(0, steps)
+        def _(c):
+            here = pl.ds(pl.multiple_of((chunk * steps + c) * wide, wide), wide)
+            part = pl.ds(pl.multiple_of(c * wide, wide), wide)
+            left = active[chunk, :, :, :, part].reshape(batch, wide)
+            acc[...] += jnp.dot(left, wd[here, :], preferred_element_type=jnp.float32)
 
     down_terms[...] = acc[...].astype(jnp.bfloat16).reshape(n_tp, piece, cols)
     down, copies = reduce_tp(down_terms, down_land, ds, dr, n_tp)
     pending += copies
     output[...] = (resid[...].astype(jnp.float32) + down).astype(jnp.bfloat16)
+    state_store.wait()
     for copy in pending:
         copy.wait_send()
 
@@ -368,19 +412,23 @@
     heads = state.shape[1]
     whole = heads * 2 * (DK + DV)
     hidden = hidden_weight.shape[1]
-    wide = min(512, hidden)
+    wide = min(512, hidden // CHUNKS)
     vmem, hbm = pl.BlockSpec(memory_space=VMEM), pl.BlockSpec(memory_space=pltpu.HBM)
 
-    def scatter_buffers(width):
+    def scatter_buffers(width, *lead):
         return [
-            VMEM((outer, inner, own, width), bf16),
-            VMEM((inner, outer, own, width), bf16),
-            VMEM((outer, own, width), bf16),
-            VMEM((outer, own, width), bf16),
+            VMEM(lead + (outer, inner, own, width), bf16),
+            VMEM(lead + (inner, outer, own, width), bf16),
+            VMEM(lead + (outer, own, width), bf16),
+            VMEM(lead + (outer, own, width), bf16),
         ]
 
-    two_in = [DMA((inner, outer)), DMA((inner, outer))]
-    two_out = [DMA((outer,)), DMA((outer,))]
+    def two_in(*lead):
+        return [DMA(lead + (inner, outer))] * 2
+
+    def two_out(*lead):
+        return [DMA(lead + (outer,))] * 2
+
     over_tp = [DMA((n_tp,)), DMA((n_tp,))]
     over_kv = [DMA((n_kv,)), DMA((n_kv,))]
     squares = [VMEM((n_kv, own, 128), f32), VMEM((n_kv, own, 128), f32)]
@@ -392,19 +440,22 @@
             jax.ShapeDtypeStruct(state.shape, f32),
         ],
         in_specs=[vmem] * 2 + [hbm] * 12,
-        out_specs=[vmem] * 2,
+        out_specs=[vmem, hbm],
         scratch_shapes=[
             VMEM(tokens.shape, bf16), VMEM((1, cols), f32), VMEM((1, cols), f32),
             VMEM((1, heads * DV), f32),
             tp_rows, VMEM((cols, whole), bf16),
         ]
-        + scatter_buffers(whole)
+        + scatter_buffers(whole - heads * DV)
+        + scatter_buffers(heads * DV)
         + squares
         + [
             VMEM((own, 2 * heads, DK), f32),
             VMEM((own, heads, DV), f32),
-            VMEM((own, heads, DV), f32),
             VMEM((own, heads * DV), f32),
+            VMEM(state.shape, f32),
+            VMEM(state.shape, f32),
+            VMEM((own, DK, 2 * heads), f32),
             VMEM((outer, inner, own, heads * DV), bf16),
             VMEM(out_weight.shape, bf16),
             VMEM(hidden_weight.shape, bf16),
@@ -412,21 +463,21 @@
             tp_rows, tp_rows, VMEM((piece, cols), bf16), tp_rows,
         ]
         + squares
-        + scatter_buffers(hidden)
+        + scatter_buffers(hidden // CHUNKS, CHUNKS)
         + [
-            VMEM((outer, inner, own, hidden), bf16),
+            VMEM((CHUNKS, outer, inner, own, hidden // CHUNKS), bf16),
             VMEM((n_tp * piece, cols), f32),
             tp_rows, tp_rows,
-            DMA((4,)), DMA((7,)), DMA((1,)),
+            DMA((4,)), DMA((7,)), DMA((2,)),
         ]
-        + over_tp + over_kv + two_in + two_out
-        + two_out + two_in
+        + over_tp + over_kv + two_in() + two_out() + two_in() + two_out()
+        + two_out() + two_in()
         + over_tp + over_tp + over_kv
-        + two_in + two_out
-        + two_out + two_in
+        + two_in(CHUNKS) + two_out(CHUNKS)
+        + two_out(CHUNKS) + two_in(CHUNKS)
         + over_tp,
         compiler_params=pltpu.CompilerParams(
-            collective_id=0, has_side_effects=True, vmem_limit_bytes=48 * 2**20
+            collective_id=0, has_side_effects=True, vmem_limit_bytes=67043328
         ),
     )(
         cosine, sine, tokens, norm_in_gain[None, :], norm_mlp_gain[None, :], head_gain[None, :],

time: 114 us -> 93.3 us (0.82); the launches traced: 112 us -> 93 us
  Pallas kernels: 93.6 us -> 81.7 us
  local copies, waits for them, and re-layouts: 17 us -> 9.15 us
    pallas_call x1, Pallas kernels: 93.6 us -> 81.7 us  [local(): pl.pallas_call(functools.partial(layer_kernel, n_kv, n_tp, inner, feature...]
    unnamed x20 -> x2, local copies, waits for them, and re-layouts: 17 us -> 9.15 us
where the time goes in v3:
time: 93.3 us; the launch traced here: 93 us
  Pallas kernels  81.7 us (88%)
  local copies, waits for them, and re-layouts  9.15 us (10%)
  other arithmetic  1.47 us (2%)
    pallas_call x1, Pallas kernels, local(): pl.pallas_call(functools.partial(layer_kernel, n_kv, n_tp, inner, feature...  81.7 us
    unnamed x2, local copies, waits for them, and re-layouts  9.15 us

profile of v3, /device:TPU:0, one launch (start us, length us, event | category | flops | bytes accessed | tf_op | source)
XLA Modules:
  0.0 93.0 jit_solution(15973017735230335922)
XLA Ops:
  0.6 0.7 convert_element_type.3
  1.3 0.1 fusion
  1.4 0.7 pad_maximum_fusion
  2.1 81.7 %shard_map.140 = (bf16[32,512]{1,0:T(8,128)(2,1)}, f32[16,4,128,256]{3,2,1,0:T(8,128)}) custom-call(f32[16,128]{1,0:T(8,128)} %get-tuple-element.5.cosine, f32[16,128]{1,0:T(8,128)} %get-tuple-element.6.sine, bf16[32,512]{1,0:T(8,128)(2,1)} %tokens_hbm.1, f32[1,512]{1,0:T(1,128)} %bitcast.4, f32[1,512]{1,0:T(1,128)} %bitcast.5, f32[1,1024]{1,0:T(1,128)} %bitcast.3, ...), custom_call_target="tpu_custom_call" | custom-call | tf_op jit(solution)/shard_map/pallas_call | solution.py:436
  83.8 1.4 %copy.17 = bf16[32,512]{1,0:T(8,128)(2,1)} copy(bf16[32,512]{1,0:T(8,128)(2,1)} %get-tuple-element.9) | data formatting | bytes 65536
  85.2 7.8 %copy.18 = f32[16,4,128,256]{3,2,1,0:T(8,128)} copy(f32[16,4,128,256]{3,2,1,0:T(8,128)} %get-tuple-element.10) | data formatting | bytes 16777216
  (1 shorter events, 0.0 us)
